TPU v7x, 128 devices: a whole 4x4x4 slice. The times are simulated.
128 devices in a mesh: rep: 16 (over z, x), fs: 4 (over y), tp: 2 (over core).
Axes of the slice: x: 4, y: 4, z: 4, core: 2. Of those that a mesh axis runs over, the one named last changes fastest.
Arguments:
- tokens_in: bfloat16 [32768, 2048], P(('rep', 'fs', 'tp')), may hold values from -6 to 6
- norm_gain: float32 [2048], replicated, may hold values from 0.1 to 1.9
- gate_weight: bfloat16 [2048, 3072], P(None, ('fs', 'tp')), may hold values from -0.125 to 0.125
- up_weight: bfloat16 [2048, 3072], P(None, ('fs', 'tp')), may hold values from -0.125 to 0.125
- down_weight: bfloat16 [3072, 2048], P(('fs', 'tp')), may hold values from -0.109375 to 0.109375
- out_grad: bfloat16 [32768, 2048], P(('rep', 'fs', 'tp')), may hold values from -24 to 24
Outputs:
- grad_in: bfloat16 [32768, 2048], P(('rep', 'fs', 'tp'))
- grad_gain: float32 [2048], replicated
- grad_gate: float32 [2048, 3072], P(None, ('fs', 'tp'))
- grad_up: float32 [2048, 3072], P(None, ('fs', 'tp'))
- grad_down: float32 [3072, 2048], P(('fs', 'tp'))
All inputs are finite; a program needn't handle non-finite values.
Results may differ from a plain program's by a relative error of at most 0.014.
Values may be sent and summed in bfloat16 or wider, within the bound.
A program may use at most 192 MiB of HBM per device.

v0:
```python
import jax
import jax.numpy as jnp
from jax import lax
from jax.sharding import PartitionSpec as P

norm_eps = 1e-06


def sent_to_all(value, axis):
    length = lax.axis_size(axis)
    return lax.all_to_all(
        jnp.broadcast_to(value[None], (length, *value.shape)), axis, 0, 0, tiled=True
    )


def taken_together(value, axis):
    return sent_to_all(value, axis).sum(axis=0)


def shards(tokens_in, norm_gain, gate_weight, up_weight, down_weight, out_grad):
    row_count = tokens_in.shape[0]
    total_tokens = row_count * lax.axis_size("rep") * lax.axis_size("fs") * lax.axis_size("tp")
    factor = float(total_tokens) ** (-0.5)
    whole_in, whole_grad = (
        lax.all_gather(tokens_in, ("fs", "tp"), axis=0, tiled=True),
        lax.all_gather(out_grad, ("fs", "tp"), axis=0, tiled=True),
    )
    floats = whole_in.astype(jnp.float32)
    inverse = lax.rsqrt(jnp.mean(floats * floats, axis=-1, keepdims=True) + norm_eps)
    unit_rows = floats * inverse
    normed = (unit_rows * norm_gain).astype(jnp.bfloat16)
    gate_pre = jnp.dot(normed, gate_weight, preferred_element_type=jnp.float32)
    up_pre = jnp.dot(normed, up_weight, preferred_element_type=jnp.float32)
    sigma = jax.nn.sigmoid(gate_pre)
    active = gate_pre * sigma
    hidden = (active * up_pre).astype(jnp.bfloat16)
    grad_hidden = 0.5 * jnp.dot(whole_grad, down_weight.T, preferred_element_type=jnp.float32)
    grad_gate_pre = (grad_hidden * up_pre * sigma * (1.0 + gate_pre * (1.0 - sigma))).astype(
        jnp.bfloat16
    )
    grad_up_pre = (grad_hidden * active).astype(jnp.bfloat16)
    result = jnp.dot(grad_gate_pre, gate_weight.T, preferred_element_type=jnp.float32)
    grad_normed = lax.psum_scatter(
        (result + jnp.dot(grad_up_pre, up_weight.T, preferred_element_type=jnp.float32)).astype(
            jnp.bfloat16
        ),
        ("fs", "tp"),
        scatter_dimension=0,
        tiled=True,
    ).astype(jnp.float32)
    local_gate = jnp.dot(normed.T, grad_gate_pre, preferred_element_type=jnp.float32)
    local_up = jnp.dot(normed.T, grad_up_pre, preferred_element_type=jnp.float32)
    local_down = jnp.dot(hidden.T, whole_grad, preferred_element_type=jnp.float32)
    summed_gate = lax.psum(local_gate.astype(jnp.bfloat16), "rep").astype(jnp.float32)
    summed_up = lax.psum(local_up.astype(jnp.bfloat16), "rep").astype(jnp.float32)
    summed_down = lax.psum(local_down.astype(jnp.bfloat16), "rep").astype(jnp.float32)
    grad_gate = summed_gate * factor
    grad_up = summed_up * factor
    grad_down = summed_down * (0.5 * factor)
    position = lax.axis_index("fs") * lax.axis_size("tp") + lax.axis_index("tp")
    own_unit = lax.dynamic_slice_in_dim(unit_rows, position * row_count, row_count, 0)
    own_inverse = lax.dynamic_slice_in_dim(inverse, position * row_count, row_count, 0)
    gain_local = jnp.sum(grad_normed * own_unit, axis=0)
    gain_partial = taken_together(gain_local, ("fs", "tp"))
    grad_gain = taken_together(gain_partial, "rep")
    scaled = grad_normed * norm_gain
    grad_in = (
        out_grad.astype(jnp.float32)
        + own_inverse * scaled
        - own_unit * own_inverse * jnp.mean(scaled * own_unit, axis=-1, keepdims=True)
    )
    return (grad_in.astype(jnp.bfloat16), grad_gain, grad_gate, grad_up, grad_down)


def solution(mesh):
    in_specs = (
        P(("rep", "fs", "tp"), None),
        P(),
        P(None, ("fs", "tp")),
        P(None, ("fs", "tp")),
        P(("fs", "tp"), None),
        P(("rep", "fs", "tp"), None),
    )
    out_specs = (
        P(("rep", "fs", "tp"), None),
        P(),
        P(None, ("fs", "tp")),
        P(None, ("fs", "tp")),
        P(("fs", "tp"), None),
    )
    return jax.shard_map(shards, mesh=mesh, in_specs=in_specs, out_specs=out_specs, check_vma=False)
```

profile of v0, /device:TPU:0, one launch (start us, length us, event | category | flops | bytes accessed | tf_op | source)
XLA Modules:
  0.0 341.8 jit_solution(17009870952825740865)
XLA Ops:
  7.2 0.0 copy-start
  7.2 0.0 all-gather.3.cloned.1.call-start
  7.2 0.0 copy-start.3
  7.2 0.7 all-gather.3.cloned.1.call-update
  7.9 0.0 all-gather.5.cloned.1.call-start
  8.0 0.7 all-gather.5.cloned.1.call-update
  8.7 0.0 copy-start.9
  8.7 0.0 all-reduce.3.cloned.1.call-start
  8.7 53.2 %all-gather.3.cloned.1.call-done = bf16[2048,2048]{1,0:T(8,128)(2,1)} async-done(((bf16[256,2048]{1,0:T(8,128)(2,1)}), bf16[2048,2048]{1,0:T(8,128)(2,1)}) %all-gather.3.cloned.1.call-update) | async-done | bytes 8388624 | tf_op jit(solution)/shard_map/all_gather | solution.py:25
  61.9 5.2 %fusion = f32[2048]{0:T(1024)S(1)} fusion(bf16[2048,2048]{1,0:T(8,128)(2,1)} %all-gather.3.cloned.1.call-done), kind=kLoop, calls=%fused_computation.2 | loop fusion | flops 12580864 | bytes 8396800 | tf_op jit(solution)/shard_map/reduce_sum | solution.py:29
  67.1 0.0 copy-done.3
  67.2 0.0 copy-done.9
  67.2 0.5 copy-done.1
  67.7 6.3 %fusion.12 = f32[2048,384]{1,0:T(8,128)} fusion(bf16[2048,384]{1,0:T(8,128)(2,1)S(1)} %copy-done.3, f32[2048]{0:T(1024)S(1)} %copy-done.9, f32[2048]{0:T(1024)S(1)} %add_rsqrt_fusion, bf16[2048,2048]{1,0:T(8,128)(2,1)S(1)} %copy-done.1), kind=kOutput, calls=%fused_computation.30 | convolution fusion | flops 3238002688 | bytes 13123584 | tf_op jit(solution)/shard_map/dot_general | solution.py:33
  74.0 6.4 %fusion.11 = f32[2048,384]{1,0:T(8,128)} fusion(bf16[2048,384]{1,0:T(8,128)(2,1)S(1)} %copy-done, f32[2048]{0:T(1024)S(1)} %copy-done.9, f32[2048]{0:T(1024)S(1)} %add_rsqrt_fusion, bf16[2048,2048]{1,0:T(8,128)(2,1)S(1)} %copy-done.1), kind=kOutput, calls=%fused_computation.29 | convolution fusion | flops 3238002688 | bytes 13123584 | tf_op jit(solution)/shard_map/dot_general | solution.py:32
  80.4 33.1 %all-gather.5.cloned.1.call-done = bf16[2048,2048]{1,0:T(8,128)(2,1)} async-done(((bf16[256,2048]{1,0:T(8,128)(2,1)}), bf16[2048,2048]{1,0:T(8,128)(2,1)}) %all-gather.5.cloned.1.call-update) | async-done | bytes 8388624 | tf_op jit(solution)/shard_map/all_gather | solution.py:26
  113.5 10.3 %convolution_convert_fusion = bf16[384,2048]{1,0:T(8,128)(2,1)} fusion(bf16[2048,2048]{1,0:T(8,128)(2,1)} %all-gather.5.cloned.1.call-done, f32[2048,384]{1,0:T(8,128)} %fusion.12, f32[2048,384]{1,0:T(8,128)} %fusion.11), kind=kOutput, calls=%fused_computation.14 | convolution fusion | flops 3226730496 | bytes 16252928 | tf_op jit(solution)/shard_map/dot_general | solution.py:53
  123.8 0.0 copy-done.12
  123.8 0.0 slice-start.1
  123.8 7.5 %multiply_convert_fusion.2 = (bf16[2048,384]{1,0:T(8,128)(2,1)S(1)}, bf16[2048,384]{1,0:T(8,128)(2,1)S(1)}) fusion(f32[2048,384]{1,0:T(8,128)} %fusion.11, f32[2048,384]{1,0:T(8,128)S(1)} %copy-done.12, bf16[2048,2048]{1,0:T(8,128)(2,1)S(1)} %copy-done.10, bf16[384,2048]{1,0:T(8,128)(2,1)S(1)} %copy-done.11), kind=kOutput, calls=%fused_computation.9 | convolution fusion | flops 3232235520 | bytes 19398656 | tf_op jit(solution)/shard_map/dot_general | solution.py:37
  131.3 0.0 copy-start.6
  131.3 0.0 copy-start.8
  131.4 6.1 %convolution_convert_fusion.1 = bf16[2048,384]{1,0:T(8,128)(2,1)} fusion(bf16[2048,384]{1,0:T(8,128)(2,1)S(1)} %get-tuple-element.10, f32[2048]{0:T(1024)S(1)} %copy-done.9, f32[2048]{0:T(1024)S(1)} %add_rsqrt_fusion, bf16[2048,2048]{1,0:T(8,128)(2,1)S(1)} %bitcast.12), kind=kOutput, calls=%fused_computation.15 | convolution fusion | flops 3238789120 | bytes 11550720 | tf_op jit(solution)/shard_map/dot_general | solution.py:52
  137.5 0.0 copy-done.6
  137.5 6.1 %convolution_convert_fusion.2 = bf16[2048,384]{1,0:T(8,128)(2,1)} fusion(bf16[2048,384]{1,0:T(8,128)(2,1)S(1)} %get-tuple-element.11, f32[2048]{0:T(1024)S(1)} %copy-done.9, f32[2048]{0:T(1024)S(1)} %add_rsqrt_fusion, bf16[2048,2048]{1,0:T(8,128)(2,1)S(1)} %bitcast.12), kind=kOutput, calls=%fused_computation.16 | convolution fusion | flops 3238789120 | bytes 11550720 | tf_op jit(solution)/shard_map/dot_general | solution.py:51
  143.5 0.0 all-reduce.3.cloned.1.call-update
  143.6 0.3 reduce-scatter.2.cloned.1.call-start
  143.8 0.0 copy-start.7
  143.8 10.1 %fusion.13 = f32[2048,2048]{1,0:T(8,128)} fusion(bf16[2048,384]{1,0:T(8,128)(2,1)} %copy-done.8, bf16[2048,384]{1,0:T(8,128)(2,1)S(1)} %copy-done), kind=kOutput, calls=%fused_computation.31 | convolution fusion | flops 3221225472 | bytes 19922944 | tf_op jit(solution)/shard_map/dot_general | solution.py:42
  153.9 10.3 %add_convert_fusion = bf16[2048,2048]{1,0:T(8,128)(2,1)} fusion(f32[2048,2048]{1,0:T(8,128)} %fusion.13, bf16[2048,384]{1,0:T(8,128)(2,1)S(1)} %copy-done.7, bf16[2048,384]{1,0:T(8,128)(2,1)S(1)} %copy-done.3), kind=kOutput, calls=%fused_computation.3 | convolution fusion | flops 3229614080 | bytes 28311552 | tf_op jit(solution)/shard_map/dot_general | solution.py:44
  164.3 0.0 reduce-scatter.2.cloned.1.call-update
  164.3 0.1 dynamic-slice.3
  164.4 10.6 %convert_multiply_fusion = f32[2048,2048]{1,0:T(8,128)} fusion(bf16[2048,2048]{1,0:T(8,128)(2,1)} %all-gather.3.cloned.1.call-done, f32[2048]{0:T(1024)S(1)} %add_rsqrt_fusion), kind=kLoop, calls=%fused_computation | loop fusion | flops 8388608 | bytes 25174016 | tf_op jit(solution)/shard_map/mul | solution.py:30
  175.0 77.3 %all-reduce.3.cloned.1.call-done = (bf16[2048,384]{1,0:T(8,128)(2,1)}, bf16[2048,384]{1,0:T(8,128)(2,1)}, bf16[384,2048]{1,0:T(8,128)(2,1)}) async-done(((bf16[2048,384]{1,0:T(8,128)(2,1)}, bf16[2048,384]{1,0:T(8,128)(2,1)}, bf16[384,2048]{1,0:T(8,128)(2,1)}), (bf16[2048,384]{1,0:T(8,128)(2,1)}, bf16[2048,384]{1,0:T(8,128)(2,1)}, bf16[384,2048]{1,0:T(8,128)(2,1)})) %all-reduce.3.cloned.1.call-update) | async-done | bytes 4718608 | tf_op jit(solution)/shard_map/psum | solution.py:54
  252.3 3.6 %convert_multiply_fusion.2 = f32[384,2048]{1,0:T(8,128)} fusion(bf16[384,2048]{1,0:T(8,128)(2,1)} %get-tuple-element.9), kind=kLoop, calls=%fused_computation.5 | loop fusion | flops 1572864 | bytes 4718592 | tf_op jit(solution)/shard_map/mul | solution.py:59
  255.9 3.3 convert_multiply_fusion.3
  259.2 47.5 %reduce-scatter.2.cloned.1.call-done = bf16[256,2048]{1,0:T(8,128)(2,1)} async-done(((bf16[2048,2048]{1,0:T(8,128)(2,1)}), bf16[256,2048]{1,0:T(8,128)(2,1)}) %reduce-scatter.2.cloned.1.call-update) | async-done | bytes 1048592 | tf_op jit(solution)/shard_map/reduce_scatter | solution.py:43
  306.7 2.6 fusion.8
  309.2 0.7 broadcast_in_dim.4
  309.9 3.4 all-to-all-start
  313.3 5.5 %all-to-all-done = f32[8,1,2048]{2,1,0:T(1,128)S(1)} async-done(((f32[8,1,2048]{2,1,0:T(1,128)}), f32[8,1,2048]{2,1,0:T(1,128)S(1)}, u32[]{:S(2)}, u32[]{:S(2)}) %all-to-all-start) | async-done | bytes 65568 | tf_op jit(solution)/shard_map/all_to_all | solution.py:11
  318.8 0.1 reduce_sum.48
  318.9 0.7 broadcast_in_dim.5
  319.6 6.9 %all-to-all-start.1 = ((f32[16,1,2048]{2,1,0:T(1,128)}), f32[16,1,2048]{2,1,0:T(1,128)S(1)}, u32[]{:S(2)}, u32[]{:S(2)}) async-start(f32[16,1,2048]{2,1,0:T(1,128)} %broadcast_in_dim.5), calls=%async_computation.2 | async-start | bytes 262144 | tf_op jit(solution)/shard_map/all_to_all | solution.py:11
  326.5 0.0 copy-done.2
  326.6 3.6 %fusion.6 = bf16[256,2048]{1,0:T(8,128)(2,1)} fusion(bf16[256,2048]{1,0:T(8,128)(2,1)} %reduce-scatter.2.cloned.1.call-done, bf16[256,2048]{1,0:T(8,128)(2,1)S(1)} %copy-done.2, f32[2048,2048]{1,0:T(8,128)} %convert_multiply_fusion, s32[]{:T(128)S(6)} %select_n.4, f32[256]{0:T(256)S(1)} %broadcast_multiply_fusion, f32[2048]{0:T(1024)S(1)} %copy-done.9, ...), kind=kLoop, calls=%fused_computation.23 | loop fusion | flops 4718592 | bytes 5253124 | tf_op jit(solution)/shard_map/convert_element_type | solution.py:72
  330.1 4.4 %all-to-all-done.1 = f32[16,1,2048]{2,1,0:T(1,128)S(1)} async-done(((f32[16,1,2048]{2,1,0:T(1,128)}), f32[16,1,2048]{2,1,0:T(1,128)S(1)}, u32[]{:S(2)}, u32[]{:S(2)}) %all-to-all-start.1) | async-done | bytes 131104 | tf_op jit(solution)/shard_map/all_to_all | solution.py:11
  334.5 0.7 reduce_sum.49
  (20 shorter events, 0.0 us)
Async XLA Ops:
  7.2 66.8 %copy-start = (bf16[2048,384]{1,0:T(8,128)(2,1)S(1)}, bf16[2048,384]{1,0:T(8,128)(2,1)}, u32[]{:S(2)}) copy-start(bf16[2048,384]{1,0:T(8,128)(2,1)} %param.8) | copy-start | bytes 4718596
  7.2 54.7 %all-gather.3.cloned.1.call-start = ((), (), s32[]{:S(2)}) async-start(), calls=%async_computation.3 | async-start | bytes 9437184 | tf_op jit(solution)/shard_map/all_gather | solution.py:25
  7.2 59.9 %copy-start.3 = (bf16[2048,384]{1,0:T(8,128)(2,1)S(1)}, bf16[2048,384]{1,0:T(8,128)(2,1)}, u32[]{:S(2)}) copy-start(bf16[2048,384]{1,0:T(8,128)(2,1)} %param.9) | copy-start | bytes 4718596
  7.9 105.6 %all-gather.5.cloned.1.call-start = ((), (), s32[]{:S(2)}) async-start(), calls=%async_computation.4 | async-start | bytes 9437184 | tf_op jit(solution)/shard_map/all_gather | solution.py:26
  8.7 58.5 %copy-start.9 = (f32[2048]{0:T(1024)S(1)}, f32[2048]{0:T(1024)}, u32[]{:S(2)}) copy-start(f32[2048]{0:T(1024)} %param.7) | copy-start | bytes 24580
  8.7 243.6 %all-reduce.3.cloned.1.call-start = ((), (), s32[]{:S(2)}) async-start(), calls=%async_computation.6 | async-start | bytes 9437184 | tf_op jit(solution)/shard_map/psum | solution.py:54
  61.9 5.8 %copy-start.1 = (bf16[2048,2048]{1,0:T(8,128)(2,1)S(1)}, bf16[2048,2048]{1,0:T(8,128)(2,1)}, u32[]{:S(2)}) copy-start(bf16[2048,2048]{1,0:T(8,128)(2,1)} %all-gather.3.cloned.1.call-done) | copy-start | bytes 25165828
  113.5 10.4 %copy-start.10 = (bf16[2048,2048]{1,0:T(8,128)(2,1)S(1)}, bf16[2048,2048]{1,0:T(8,128)(2,1)}, u32[]{:S(2)}) copy-start(bf16[2048,2048]{1,0:T(8,128)(2,1)} %all-gather.5.cloned.1.call-done) | copy-start | bytes 25165828
  113.5 10.4 %copy-start.11 = (bf16[384,2048]{1,0:T(8,128)(2,1)S(1)}, bf16[384,2048]{1,0:T(8,128)(2,1)}, u32[]{:S(2)}) copy-start(bf16[384,2048]{1,0:T(8,128)(2,1)} %param.10) | copy-start | bytes 4718596
  113.5 10.4 %copy-start.12 = (f32[2048,384]{1,0:T(8,128)S(1)}, f32[2048,384]{1,0:T(8,128)}, u32[]{:S(2)}) copy-start(f32[2048,384]{1,0:T(8,128)} %fusion.12) | copy-start | bytes 9437188
  113.5 17.9 %slice-start = ((s8[8388608]{0:T(1024)(128)(4,1)}), s8[4194304]{0:T(1024)(128)(4,1)S(1)}, s32[]{:S(2)}) async-start(s8[8388608]{0:T(1024)(128)(4,1)} %bitcast.11), calls=%async_computation.7 | async-start | bytes 8388608
  123.8 7.5 %slice-start.1 = ((s8[8388608]{0:T(1024)(128)(4,1)}), s8[4194304]{0:T(1024)(128)(4,1)S(1)}, s32[]{:S(2)}) async-start(s8[8388608]{0:T(1024)(128)(4,1)} %bitcast.11), calls=%async_computation.8 | async-start | bytes 8388608
  131.3 6.1 %copy-start.6 = (bf16[2048,384]{1,0:T(8,128)(2,1)}, bf16[2048,384]{1,0:T(8,128)(2,1)S(1)}, u32[]{:S(2)}) copy-start(bf16[2048,384]{1,0:T(8,128)(2,1)S(1)} %get-tuple-element.10) | copy-start | bytes 4718596
  131.3 6.1 %copy-start.8 = (bf16[2048,384]{1,0:T(8,128)(2,1)}, bf16[2048,384]{1,0:T(8,128)(2,1)S(1)}, u32[]{:S(2)}) copy-start(bf16[2048,384]{1,0:T(8,128)(2,1)S(1)} %get-tuple-element.11) | copy-start | bytes 4718596
  143.6 163.1 %reduce-scatter.2.cloned.1.call-start = ((), (), s32[]{:S(2)}) async-start(), calls=%async_computation.5 | async-start | bytes 9437184 | tf_op jit(solution)/shard_map/reduce_scatter | solution.py:43
  143.8 10.1 %copy-start.7 = (bf16[2048,384]{1,0:T(8,128)(2,1)S(1)}, bf16[2048,384]{1,0:T(8,128)(2,1)}, u32[]{:S(2)}) copy-start(bf16[2048,384]{1,0:T(8,128)(2,1)} %copy-done.6) | copy-start | bytes 4718596
  252.3 3.6 %copy-start.4 = (bf16[2048,384]{1,0:T(8,128)(2,1)S(1)}, bf16[2048,384]{1,0:T(8,128)(2,1)}, u32[]{:S(2)}) copy-start(bf16[2048,384]{1,0:T(8,128)(2,1)} %get-tuple-element.7) | copy-start | bytes 4718596
  252.3 3.6 %copy-start.5 = (bf16[2048,384]{1,0:T(8,128)(2,1)S(1)}, bf16[2048,384]{1,0:T(8,128)(2,1)}, u32[]{:S(2)}) copy-start(bf16[2048,384]{1,0:T(8,128)(2,1)} %get-tuple-element.8) | copy-start | bytes 4718596
  259.1 67.4 %copy-start.2 = (bf16[256,2048]{1,0:T(8,128)(2,1)S(1)}, bf16[256,2048]{1,0:T(8,128)(2,1)}, u32[]{:S(2)}) copy-start(bf16[256,2048]{1,0:T(8,128)(2,1)} %param.11) | copy-start | bytes 3145732
  309.9 8.9 %all-to-all-start = ((f32[8,1,2048]{2,1,0:T(1,128)}), f32[8,1,2048]{2,1,0:T(1,128)S(1)}, u32[]{:S(2)}, u32[]{:S(2)}) async-start(f32[8,1,2048]{2,1,0:T(1,128)} %broadcast_in_dim.4), calls=%async_computation.1 | async-start | bytes 131072 | tf_op jit(solution)/shard_map/all_to_all | solution.py:11
  319.6 14.9 %all-to-all-start.1 = ((f32[16,1,2048]{2,1,0:T(1,128)}), f32[16,1,2048]{2,1,0:T(1,128)S(1)}, u32[]{:S(2)}, u32[]{:S(2)}) async-start(f32[16,1,2048]{2,1,0:T(1,128)} %broadcast_in_dim.5), calls=%async_computation.2 | async-start | bytes 262144 | tf_op jit(solution)/shard_map/all_to_all | solution.py:11
Sparse Core Ops, SparseCore 0:
  9.7 52.1 all-gather.2
  63.6 49.8 all-gather.4
  143.7 108.5 all-reduce.2
  254.5 52.1 reduce-scatter.1
where the time goes:
time: 342 us
  waiting for transfers between devices  222 us (65%)
  matrix products  63.1 us (18%)
  other arithmetic  29.6 us (9%)
  between operations  13.9 us (4%)
  starting transfers between devices  10.7 us (3%)
    psum x1, waiting for transfers between devices, shards(): lax.psum(local_gate.astype(jnp.bfloat16), 'rep').astype(jnp.float32)  77.3 us
    all_gather x1, waiting for transfers between devices, shards(): lax.all_gather(tokens_in, ('fs', 'tp'), axis=0, tiled=True)  53.2 us
    reduce_scatter x1, waiting for transfers between devices, shards(): lax.psum_scatter((result + jnp.dot(grad_up_pre, up_weight.T, preferred_el...  47.5 us
    all_gather x1, waiting for transfers between devices, shards(): lax.all_gather(out_grad, ('fs', 'tp'), axis=0, tiled=True)  33.1 us
    mul x1, other arithmetic, shards(): unit_rows = floats * inverse  10.6 us
    dot_general x1, matrix products, shards(): jnp.dot(hidden.T, whole_grad, preferred_element_type=jnp.float32)  10.3 us
    dot_general x1, matrix products, shards(): jnp.dot(grad_up_pre, up_weight.T, preferred_element_type=jnp.float32)  10.3 us
    all_to_all x2, starting transfers between devices, sent_to_all(): lax.all_to_all(jnp.broadcast_to(value[None], (length, *value.shape)), axi...  10.3 us
  transfers between devices with their start and end apart: 6, of which 6 were waited for; matrix products, arithmetic and copies ran while one was open for 17% of the time, Pallas kernels for 0%

commit v1 on v0

--- a/solution.py
+++ b/solution.py
@@ -51,7 +51,12 @@
     local_gate = jnp.dot(normed.T, grad_gate_pre, preferred_element_type=jnp.float32)
     local_up = jnp.dot(normed.T, grad_up_pre, preferred_element_type=jnp.float32)
     local_down = jnp.dot(hidden.T, whole_grad, preferred_element_type=jnp.float32)
-    summed_gate = lax.psum(local_gate.astype(jnp.bfloat16), "rep").astype(jnp.float32)
+
+    def _take_matrix(arr_in, group_axis):
+        all_rows = jnp.sum(jax.lax.all_gather(arr_in, axis_name=group_axis), axis=0)
+        return all_rows
+
+    summed_gate = _take_matrix(local_gate.astype(jnp.bfloat16), "rep").astype(jnp.float32)
     summed_up = lax.psum(local_up.astype(jnp.bfloat16), "rep").astype(jnp.float32)
     summed_down = lax.psum(local_down.astype(jnp.bfloat16), "rep").astype(jnp.float32)
     grad_gate = summed_gate * factor

time: 342 us -> 470 us (1.37)
  waiting for transfers between devices: 222 us -> 330 us
  other arithmetic: 29.6 us -> 43 us
    all_gather x0 -> x1, waiting for transfers between devices: none -> 128 us  [_take_matrix(): all_rows = jnp.sum(jax.lax.all_gather(arr_in, axis_name=group_axis), axis=0)]
    psum x1, waiting for transfers between devices: 77.3 us -> 54.5 us  [shards(): lax.psum(local_up.astype(jnp.bfloat16), 'rep').astype(jnp.float32)]
    reduce_sum x0 -> x1, other arithmetic: none -> 13.2 us  [_take_matrix(): all_rows = jnp.sum(jax.lax.all_gather(arr_in, axis_name=group_axis), axis=0)]
  transfers between devices with their start and end apart: 6 -> 7, of which waited for: 6 -> 7; matrix products, arithmetic and copies ran while one was open for 17% -> 15% of each run, Pallas kernels for 0% -> 0%
where the time goes in v1:
time: 470 us; the launch traced here: 469 us
  waiting for transfers between devices  330 us (70%)
  matrix products  67.3 us (14%)
  other arithmetic  43 us (9%)
  between operations  13.9 us (3%)
  starting transfers between devices  10.7 us (2%)
    all_gather x1, waiting for transfers between devices, _take_matrix(): all_rows = jnp.sum(jax.lax.all_gather(arr_in, axis_name=group_axis), axis=0)  128 us
    psum x1, waiting for transfers between devices, shards(): lax.psum(local_up.astype(jnp.bfloat16), 'rep').astype(jnp.float32)  54.5 us
    all_gather x1, waiting for transfers between devices, shards(): lax.all_gather(tokens_in, ('fs', 'tp'), axis=0, tiled=True)  53.2 us
    reduce_scatter x1, waiting for transfers between devices, shards(): lax.psum_scatter((result + jnp.dot(grad_up_pre, up_weight.T, preferred_el...  48.1 us
    all_gather x1, waiting for transfers between devices, shards(): lax.all_gather(out_grad, ('fs', 'tp'), axis=0, tiled=True)  33.1 us
    reduce_sum x1, other arithmetic, _take_matrix(): all_rows = jnp.sum(jax.lax.all_gather(arr_in, axis_name=group_axis), axis=0)  13.2 us
    all_to_all x2, waiting for transfers between devices, sent_to_all(): lax.all_to_all(jnp.broadcast_to(value[None], (length, *value.shape)), axi...  11.9 us
    mul x1, other arithmetic, shards(): unit_rows = floats * inverse  10.4 us
  transfers between devices with their start and end apart: 7, of which 7 were waited for; matrix products, arithmetic and copies ran while one was open for 15% of the time, Pallas kernels for 0%

profile of v1, /device:TPU:0, one launch (start us, length us, event | category | flops | bytes accessed | tf_op | source)
XLA Modules:
  0.0 468.9 jit_solution(5163309298973068380)
XLA Ops:
  7.2 0.0 copy-start
  7.2 0.0 all-gather.5.cloned.1.call-start
  7.2 0.0 copy-start.5
  7.2 0.7 all-gather.5.cloned.1.call-update
  7.9 0.0 all-gather.7.cloned.1.call-start
  8.0 0.7 all-gather.7.cloned.1.call-update
  8.7 0.0 all-reduce.3.cloned.1.call-start
  8.7 53.2 %all-gather.5.cloned.1.call-done = bf16[2048,2048]{1,0:T(8,128)(2,1)} async-done(((bf16[256,2048]{1,0:T(8,128)(2,1)}), bf16[2048,2048]{1,0:T(8,128)(2,1)}) %all-gather.5.cloned.1.call-update) | async-done | bytes 8388624 | tf_op jit(solution)/shard_map/all_gather | solution.py:25
  61.9 5.2 %fusion = f32[2048]{0:T(1024)S(1)} fusion(bf16[2048,2048]{1,0:T(8,128)(2,1)} %all-gather.5.cloned.1.call-done), kind=kLoop, calls=%fused_computation.2 | loop fusion | flops 12580864 | bytes 8396800 | tf_op jit(solution)/shard_map/reduce_sum | solution.py:29
  67.1 0.0 copy-done.5
  67.2 0.5 copy-done.2
  67.7 6.4 %fusion.12 = f32[2048,384]{1,0:T(8,128)} fusion(bf16[2048,384]{1,0:T(8,128)(2,1)S(1)} %copy-done.5, f32[2048]{0:T(1024)S(1)} %copy-done.10, f32[2048]{0:T(1024)S(1)} %add_rsqrt_fusion, bf16[2048,2048]{1,0:T(8,128)(2,1)S(1)} %copy-done.2), kind=kOutput, calls=%fused_computation.30 | convolution fusion | flops 3238002688 | bytes 13123584 | tf_op jit(solution)/shard_map/dot_general | solution.py:33
  74.0 6.3 %fusion.11 = f32[2048,384]{1,0:T(8,128)} fusion(bf16[2048,384]{1,0:T(8,128)(2,1)S(1)} %copy-done, f32[2048]{0:T(1024)S(1)} %copy-done.10, f32[2048]{0:T(1024)S(1)} %add_rsqrt_fusion, bf16[2048,2048]{1,0:T(8,128)(2,1)S(1)} %copy-done.2), kind=kOutput, calls=%fused_computation.29 | convolution fusion | flops 3238002688 | bytes 13123584 | tf_op jit(solution)/shard_map/dot_general | solution.py:32
  80.4 33.1 %all-gather.7.cloned.1.call-done = bf16[2048,2048]{1,0:T(8,128)(2,1)} async-done(((bf16[256,2048]{1,0:T(8,128)(2,1)}), bf16[2048,2048]{1,0:T(8,128)(2,1)}) %all-gather.7.cloned.1.call-update) | async-done | bytes 8388624 | tf_op jit(solution)/shard_map/all_gather | solution.py:26
  113.5 10.4 %convolution_convert_fusion = bf16[384,2048]{1,0:T(8,128)(2,1)} fusion(bf16[2048,2048]{1,0:T(8,128)(2,1)} %all-gather.7.cloned.1.call-done, f32[2048,384]{1,0:T(8,128)} %fusion.12, f32[2048,384]{1,0:T(8,128)} %fusion.11), kind=kOutput, calls=%fused_computation.14 | convolution fusion | flops 3226730496 | bytes 16252928 | tf_op jit(solution)/shard_map/dot_general | solution.py:53
  123.9 0.0 slice-start.1
  123.9 8.3 %multiply_convert_fusion.2 = (bf16[2048,384]{1,0:T(8,128)(2,1)S(1)}, bf16[2048,384]{1,0:T(8,128)(2,1)}) fusion(f32[2048,384]{1,0:T(8,128)} %fusion.11, f32[2048,384]{1,0:T(8,128)S(1)} %copy-done.13, bf16[2048,2048]{1,0:T(8,128)(2,1)S(1)} %copy-done.11, bf16[384,2048]{1,0:T(8,128)(2,1)S(1)} %copy-done.12), kind=kOutput, calls=%fused_computation.9 | convolution fusion | flops 3232235520 | bytes 19398656 | tf_op jit(solution)/shard_map/dot_general | solution.py:37
  132.2 1.1 copy-done.7
  133.3 6.1 %convolution_convert_fusion.1 = bf16[2048,384]{1,0:T(8,128)(2,1)} fusion(bf16[2048,384]{1,0:T(8,128)(2,1)S(1)} %get-tuple-element.9, f32[2048]{0:T(1024)S(1)} %copy-done.10, f32[2048]{0:T(1024)S(1)} %add_rsqrt_fusion, bf16[2048,2048]{1,0:T(8,128)(2,1)S(1)} %bitcast.13), kind=kOutput, calls=%fused_computation.15 | convolution fusion | flops 3238789120 | bytes 11550720 | tf_op jit(solution)/shard_map/dot_general | solution.py:52
  139.4 0.0 all-reduce.3.cloned.1.call-update
  139.4 0.0 reduce-scatter.2.cloned.1.call-start
  139.5 0.0 copy-start.8
  139.5 9.9 %fusion.13 = f32[2048,2048]{1,0:T(8,128)} fusion(bf16[2048,384]{1,0:T(8,128)(2,1)} %get-tuple-element.10, bf16[2048,384]{1,0:T(8,128)(2,1)S(1)} %copy-done), kind=kOutput, calls=%fused_computation.31 | convolution fusion | flops 3221225472 | bytes 19922944 | tf_op jit(solution)/shard_map/dot_general | solution.py:42
  149.4 10.3 %add_convert_fusion = bf16[2048,2048]{1,0:T(8,128)(2,1)} fusion(f32[2048,2048]{1,0:T(8,128)} %fusion.13, bf16[2048,384]{1,0:T(8,128)(2,1)S(1)} %copy-done.8, bf16[2048,384]{1,0:T(8,128)(2,1)S(1)} %copy-done.5), kind=kOutput, calls=%fused_computation.3 | convolution fusion | flops 3229614080 | bytes 28311552 | tf_op jit(solution)/shard_map/dot_general | solution.py:44
  159.7 0.0 reduce-scatter.2.cloned.1.call-update
  159.7 0.3 all-gather.9.cloned.1.call-start
  160.0 1.2 copy-done.6
  161.1 9.6 %convolution_convert_fusion.2 = bf16[2048,384]{1,0:T(8,128)(2,1)} fusion(bf16[2048,384]{1,0:T(8,128)(2,1)S(1)} %copy-done.6, f32[2048]{0:T(1024)S(1)} %copy-done.10, f32[2048]{0:T(1024)S(1)} %add_rsqrt_fusion, bf16[2048,2048]{1,0:T(8,128)(2,1)} %all-gather.5.cloned.1.call-done), kind=kOutput, calls=%fused_computation.16 | convolution fusion | flops 3238789120 | bytes 11550720 | tf_op jit(solution)/shard_map/dot_general | solution.py:51
  170.8 0.0 all-gather.9.cloned.1.call-update
  170.8 0.1 dynamic-slice.3
  170.9 10.4 %convert_multiply_fusion = f32[2048,2048]{1,0:T(8,128)} fusion(bf16[2048,2048]{1,0:T(8,128)(2,1)} %all-gather.5.cloned.1.call-done, f32[2048]{0:T(1024)S(1)} %add_rsqrt_fusion), kind=kLoop, calls=%fused_computation | loop fusion | flops 8388608 | bytes 25174016 | tf_op jit(solution)/shard_map/mul | solution.py:30
  181.3 54.5 %all-reduce.3.cloned.1.call-done = (bf16[2048,384]{1,0:T(8,128)(2,1)}, bf16[384,2048]{1,0:T(8,128)(2,1)}) async-done(((bf16[2048,384]{1,0:T(8,128)(2,1)}, bf16[384,2048]{1,0:T(8,128)(2,1)}), (bf16[2048,384]{1,0:T(8,128)(2,1)}, bf16[384,2048]{1,0:T(8,128)(2,1)})) %all-reduce.3.cloned.1.call-update) | async-done | bytes 3145744 | tf_op jit(solution)/shard_map/psum | solution.py:60
  235.8 3.6 convert_multiply_fusion.2
  239.3 1.9 convert_multiply_fusion.3
  241.3 48.1 %reduce-scatter.2.cloned.1.call-done = bf16[256,2048]{1,0:T(8,128)(2,1)} async-done(((bf16[2048,2048]{1,0:T(8,128)(2,1)}), bf16[256,2048]{1,0:T(8,128)(2,1)}) %reduce-scatter.2.cloned.1.call-update) | async-done | bytes 1048592 | tf_op jit(solution)/shard_map/reduce_scatter | solution.py:43
  289.4 2.6 fusion.8
  292.0 0.7 broadcast_in_dim.4
  292.7 3.4 all-to-all-start
  296.0 5.5 %all-to-all-done = f32[8,1,2048]{2,1,0:T(1,128)S(1)} async-done(((f32[8,1,2048]{2,1,0:T(1,128)}), f32[8,1,2048]{2,1,0:T(1,128)S(1)}, u32[]{:S(2)}, u32[]{:S(2)}) %all-to-all-start) | async-done | bytes 65568 | tf_op jit(solution)/shard_map/all_to_all | solution.py:11
  301.6 0.1 reduce_sum.60
  301.6 0.7 broadcast_in_dim.5
  302.3 6.9 %all-to-all-start.1 = ((f32[16,1,2048]{2,1,0:T(1,128)}), f32[16,1,2048]{2,1,0:T(1,128)S(1)}, u32[]{:S(2)}, u32[]{:S(2)}) async-start(f32[16,1,2048]{2,1,0:T(1,128)} %broadcast_in_dim.5), calls=%async_computation.2 | async-start | bytes 262144 | tf_op jit(solution)/shard_map/all_to_all | solution.py:11
  309.3 3.3 fusion.6
  312.6 6.3 %all-to-all-done.1 = f32[16,1,2048]{2,1,0:T(1,128)S(1)} async-done(((f32[16,1,2048]{2,1,0:T(1,128)}), f32[16,1,2048]{2,1,0:T(1,128)S(1)}, u32[]{:S(2)}, u32[]{:S(2)}) %all-to-all-start.1) | async-done | bytes 131104 | tf_op jit(solution)/shard_map/all_to_all | solution.py:11
  318.9 0.7 reduce_sum.61
  319.6 127.6 %all-gather.9.cloned.1.call-done = bf16[32768,384]{1,0:T(8,128)(2,1)} async-done(((bf16[2048,384]{1,0:T(8,128)(2,1)}), bf16[32768,384]{1,0:T(8,128)(2,1)}) %all-gather.9.cloned.1.call-update) | async-done | bytes 25165840 | tf_op jit(solution)/shard_map/all_gather | solution.py:56
  447.2 13.2 %reduce_sum.62 = bf16[2048,384]{1,0:T(8,128)(2,1)S(1)} reduce(bf16[16,2048,384]{2,1,0:T(8,128)(2,1)} %bitcast.14, bf16[]{:T(256)} %constant.32.clone.1), dimensions={0}, to_apply=%region_6.0 | reduce | flops 11796480 | bytes 26738690 | tf_op jit(solution)/shard_map/reduce_sum | solution.py:56
  460.4 1.9 convert_multiply_fusion.4
  (27 shorter events, 0.1 us)
Async XLA Ops:
  7.2 66.9 %copy-start = (bf16[2048,384]{1,0:T(8,128)(2,1)S(1)}, bf16[2048,384]{1,0:T(8,128)(2,1)}, u32[]{:S(2)}) copy-start(bf16[2048,384]{1,0:T(8,128)(2,1)} %param.8) | copy-start | bytes 4718596
  7.2 54.7 %all-gather.5.cloned.1.call-start = ((), (), s32[]{:S(2)}) async-start(), calls=%async_computation.3 | async-start | bytes 9437184 | tf_op jit(solution)/shard_map/all_gather | solution.py:25
  7.2 59.9 %copy-start.5 = (bf16[2048,384]{1,0:T(8,128)(2,1)S(1)}, bf16[2048,384]{1,0:T(8,128)(2,1)}, u32[]{:S(2)}) copy-start(bf16[2048,384]{1,0:T(8,128)(2,1)} %param.9) | copy-start | bytes 4718596
  7.9 105.6 %all-gather.7.cloned.1.call-start = ((), (), s32[]{:S(2)}) async-start(), calls=%async_computation.4 | async-start | bytes 9437184 | tf_op jit(solution)/shard_map/all_gather | solution.py:26
  8.7 58.5 %copy-start.10 = (f32[2048]{0:T(1024)S(1)}, f32[2048]{0:T(1024)}, u32[]{:S(2)}) copy-start(f32[2048]{0:T(1024)} %param.7) | copy-start | bytes 24580
  8.7 227.1 %all-reduce.3.cloned.1.call-start = ((), (), s32[]{:S(2)}) async-start(), calls=%async_computation.7 | async-start | bytes 6291456 | tf_op jit(solution)/shard_map/psum | solution.py:60
  61.9 5.8 %copy-start.2 = (bf16[2048,2048]{1,0:T(8,128)(2,1)S(1)}, bf16[2048,2048]{1,0:T(8,128)(2,1)}, u32[]{:S(2)}) copy-start(bf16[2048,2048]{1,0:T(8,128)(2,1)} %all-gather.5.cloned.1.call-done) | copy-start | bytes 25165828
  113.5 10.4 %copy-start.11 = (bf16[2048,2048]{1,0:T(8,128)(2,1)S(1)}, bf16[2048,2048]{1,0:T(8,128)(2,1)}, u32[]{:S(2)}) copy-start(bf16[2048,2048]{1,0:T(8,128)(2,1)} %all-gather.7.cloned.1.call-done) | copy-start | bytes 25165828
  113.5 10.4 %copy-start.12 = (bf16[384,2048]{1,0:T(8,128)(2,1)S(1)}, bf16[384,2048]{1,0:T(8,128)(2,1)}, u32[]{:S(2)}) copy-start(bf16[384,2048]{1,0:T(8,128)(2,1)} %param.10) | copy-start | bytes 4718596
  113.5 10.4 %copy-start.13 = (f32[2048,384]{1,0:T(8,128)S(1)}, f32[2048,384]{1,0:T(8,128)}, u32[]{:S(2)}) copy-start(f32[2048,384]{1,0:T(8,128)} %fusion.12) | copy-start | bytes 9437188
  113.5 19.9 %slice-start = ((s8[8388608]{0:T(1024)(128)(4,1)}), s8[4194304]{0:T(1024)(128)(4,1)S(1)}, s32[]{:S(2)}) async-start(s8[8388608]{0:T(1024)(128)(4,1)} %bitcast.12), calls=%async_computation.8 | async-start | bytes 8388608
  123.9 9.5 %slice-start.1 = ((s8[8388608]{0:T(1024)(128)(4,1)}), s8[4194304]{0:T(1024)(128)(4,1)S(1)}, s32[]{:S(2)}) async-start(s8[8388608]{0:T(1024)(128)(4,1)} %bitcast.12), calls=%async_computation.9 | async-start | bytes 8388608
  132.2 1.1 copy-start.7
  139.4 149.9 %reduce-scatter.2.cloned.1.call-start = ((), (), s32[]{:S(2)}) async-start(), calls=%async_computation.5 | async-start | bytes 9437184 | tf_op jit(solution)/shard_map/reduce_scatter | solution.py:43
  139.5 9.9 %copy-start.8 = (bf16[2048,384]{1,0:T(8,128)(2,1)S(1)}, bf16[2048,384]{1,0:T(8,128)(2,1)}, u32[]{:S(2)}) copy-start(bf16[2048,384]{1,0:T(8,128)(2,1)} %copy-done.7) | copy-start | bytes 4718596
  159.7 1.4 copy-start.6
  159.7 287.5 %all-gather.9.cloned.1.call-start = ((), (), s32[]{:S(2)}) async-start(), calls=%async_computation.6 | async-start | bytes 26738688 | tf_op jit(solution)/shard_map/all_gather | solution.py:56
  235.8 3.6 copy-start.9
  239.3 70.0 %copy-start.3 = (bf16[256,2048]{1,0:T(8,128)(2,1)S(1)}, bf16[256,2048]{1,0:T(8,128)(2,1)}, u32[]{:S(2)}) copy-start(bf16[256,2048]{1,0:T(8,128)(2,1)} %param.11) | copy-start | bytes 3145732
  289.3 20.0 %copy-start.4 = (bf16[256,2048]{1,0:T(8,128)(2,1)S(1)}, bf16[256,2048]{1,0:T(8,128)(2,1)}, u32[]{:S(2)}) copy-start(bf16[256,2048]{1,0:T(8,128)(2,1)} %reduce-scatter.2.cloned.1.call-done) | copy-start | bytes 3145732
  292.7 8.9 %all-to-all-start = ((f32[8,1,2048]{2,1,0:T(1,128)}), f32[8,1,2048]{2,1,0:T(1,128)S(1)}, u32[]{:S(2)}, u32[]{:S(2)}) async-start(f32[8,1,2048]{2,1,0:T(1,128)} %broadcast_in_dim.4), calls=%async_computation.1 | async-start | bytes 131072 | tf_op jit(solution)/shard_map/all_to_all | solution.py:11
  302.3 16.6 %all-to-all-start.1 = ((f32[16,1,2048]{2,1,0:T(1,128)}), f32[16,1,2048]{2,1,0:T(1,128)S(1)}, u32[]{:S(2)}, u32[]{:S(2)}) async-start(f32[16,1,2048]{2,1,0:T(1,128)} %broadcast_in_dim.5), calls=%async_computation.2 | async-start | bytes 262144 | tf_op jit(solution)/shard_map/all_to_all | solution.py:11
  447.2 15.2 %copy-start.1 = (bf16[2048,384]{1,0:T(8,128)(2,1)S(1)}, bf16[2048,384]{1,0:T(8,128)(2,1)}, u32[]{:S(2)}) copy-start(bf16[2048,384]{1,0:T(8,128)(2,1)} %param.8) | copy-start | bytes 4718596
Sparse Core Ops, SparseCore 0:
  9.7 52.1 all-gather.4
  63.6 49.8 all-gather.6
  139.6 96.1 all-reduce.2
  238.0 51.2 reduce-scatter.1
  291.9 155.2 all-gather.8
